TPU v7x, 32 devices: a whole 2x2x4 slice. The times are simulated.
32 devices in a mesh: kv: 4 (over y, x), tp: 8 (over z, core).
Axes of the slice: x: 2, y: 2, z: 4, core: 2. Of those that a mesh axis runs over, the one named last changes fastest.
Arguments:
- tokens: bfloat16 [32, 4096], P(None, ('kv', 'tp')), may hold values from -60 to 60, as said below
- gain_mix: float32 [4096], replicated, may hold values from 0.1 to 1.9
- w_query: bfloat16 [4096, 4096], P('kv', 'tp'), may hold values from -0.09375 to 0.09375
- w_key: bfloat16 [4096, 4096], P('kv', 'tp'), may hold values from -0.75 to 0.75
- w_value: bfloat16 [4096, 4096], P('kv', 'tp'), may hold values from -0.09375 to 0.09375
- w_outgate: bfloat16 [4096, 4096], P('kv', 'tp'), may hold values from -0.09375 to 0.09375
- w_gates: bfloat16 [4096, 32], P('kv'), may hold values from -0.09375 to 0.09375
- forget_bias: float32 [16], replicated, may hold values from 0 to 4
- cell_state: float32 [32, 4096, 256], P('kv', 'tp'), may hold values from -1.5 to 1.5
- norm_state: float32 [32, 16, 256], P('kv'), may hold values from -1.5 to 1.5
- max_state: float32 [32, 16], P('kv'), may hold values from -1 to 2
- gain_group: float32 [4096], replicated, may hold values from 0.1 to 1.9
- w_mix: bfloat16 [4096, 4096], P('tp', 'kv'), may hold values from -0.125 to 0.125
- gain_ffn: float32 [4096], replicated, may hold values from 0.1 to 1.9
- w_up: bfloat16 [4096, 16384], P('kv', 'tp'), may hold values from -0.09375 to 0.09375
- w_down: bfloat16 [16384, 4096], P('tp', 'kv'), may hold values from -0.0625 to 0.0625
Outputs:
- layer_out: bfloat16 [32, 4096], P(None, ('kv', 'tp'))
- cell_next: float32 [32, 4096, 256], P('kv', 'tp')
- norm_next: float32 [32, 16, 256], P('kv')
- max_next: float32 [32, 16], P('kv')
Inputs may be any that keep to these rules, and one draw needn't show every extreme that they name: `tokens`: finite activations.
All inputs are finite; a program needn't handle non-finite values.
Results may differ from a plain program's by a relative error of at most 0.019.
Values may be sent and summed in bfloat16 or wider, within the bound.
A program may use at most 64 MiB of HBM per device.

v0:
```python
import math

import jax
import jax.numpy as jnp
from jax import lax
from jax.sharding import PartitionSpec as P

EPSILON = 1e-06


def per_device(
    tokens,
    gain_mix,
    w_query,
    w_key,
    w_value,
    w_outgate,
    w_gates,
    forget_bias,
    cell_state,
    norm_state,
    max_state,
    gain_group,
    w_mix,
    gain_ffn,
    w_up,
    w_down,
):
    f32 = jnp.float32
    bf16 = jnp.bfloat16
    exact = lax.Precision.HIGHEST
    width = gain_mix.shape[0]
    kv_index = lax.axis_index("kv")
    tp_index = lax.axis_index("tp")
    tokf = tokens.astype(f32)
    block_rows = lax.all_gather(tokens, "tp", axis=1, tiled=True)
    block = block_rows.shape[1]
    blockf = block_rows.astype(f32)
    gain_block = lax.dynamic_slice_in_dim(gain_mix, kv_index * block, block)
    normed = (blockf * gain_block).astype(bf16)
    partials = tuple(
        (
            jnp.dot(normed, weight, preferred_element_type=f32)
            for weight in (w_query, w_key, w_value, w_outgate, w_gates)
        )
    )
    partials = partials + (jnp.sum(blockf * blockf, axis=1),)
    summed = lax.psum_scatter(partials, "kv", scatter_dimension=0, tiled=True)
    seqs = summed[0].shape[0]
    seq_squares = summed[5]
    scale_in = lax.rsqrt(seq_squares / width + EPSILON)[:, None]
    query_part = (summed[0] * scale_in).astype(bf16)
    key_part = (summed[1] * scale_in).astype(bf16)
    values = summed[2] * scale_in
    gate_out = summed[3] * scale_in
    gates = summed[4] * scale_in
    query_all, key_all = (
        lax.all_gather(query_part, "tp", axis=1, tiled=True),
        lax.all_gather(key_part, "tp", axis=1, tiled=True),
    )
    heads = forget_bias.shape[0]
    head_dim = cell_state.shape[2]
    value_rows = cell_state.shape[1]
    queryf = query_all.astype(f32).reshape(seqs, heads, head_dim)
    keyf = key_all.astype(f32).reshape(seqs, heads, head_dim) / math.sqrt(head_dim)
    gate_in = gates[:, :heads]
    log_forget = jax.nn.log_sigmoid(gates[:, heads:] + forget_bias)
    max_next = jnp.maximum(log_forget + max_state, gate_in)
    decay = jnp.exp(log_forget + max_state - max_next)
    inflow = jnp.exp(gate_in - max_next)
    norm_next = decay[..., None] * norm_state + inflow[..., None] * keyf
    denom_heads = jnp.maximum(jnp.abs(jnp.sum(norm_next * queryf, axis=2)), 1.0)
    row_ids = tp_index * value_rows + jnp.arange(value_rows)
    select = (row_ids[:, None] // head_dim == jnp.arange(heads)[None, :]).astype(f32)
    query_rows = jnp.einsum("shd,rh->srd", queryf, select, precision=exact)
    key_rows = jnp.einsum("shd,rh->srd", keyf, select, precision=exact)
    decay_rows = jnp.einsum("sh,rh->sr", decay, select, precision=exact)
    inflow_rows = jnp.einsum("sh,rh->sr", inflow, select, precision=exact)
    denom_rows = jnp.einsum("sh,rh->sr", denom_heads, select, precision=exact)
    cell_next = (
        decay_rows[:, :, None] * cell_state
        + inflow_rows[:, :, None] * values[:, :, None] * key_rows
    )
    numer = jnp.sum(cell_next * query_rows, axis=2)
    cell_read = (jax.nn.sigmoid(gate_out) * (numer / denom_rows)).astype(bf16)
    read_rows = lax.all_gather(cell_read, "kv", axis=0, tiled=True)
    readf = read_rows.astype(f32)
    group_total = lax.psum(jnp.sum(readf * readf, axis=1), "tp")
    scale_group = lax.rsqrt(group_total / (heads * head_dim) + EPSILON)[:, None]
    gain_rows = lax.dynamic_slice_in_dim(gain_group, tp_index * value_rows, value_rows)
    grouped = (readf * gain_rows).astype(bf16)
    mix_terms = jnp.dot(grouped, w_mix, preferred_element_type=f32)
    mix_summed = lax.psum_scatter(mix_terms, "tp", scatter_dimension=1, tiled=True)
    mixed = (tokf + mix_summed * scale_group).astype(bf16)
    ffn_block = w_up.shape[0]
    piece = lax.all_gather(mixed, "tp", axis=1, tiled=True)
    count = piece.shape[1]
    piecef = piece.astype(f32)
    gain_piece = lax.dynamic_slice_in_dim(gain_ffn, kv_index * ffn_block, count)
    normed_piece = (piecef * gain_piece).astype(bf16)
    up_part = jnp.dot(normed_piece, w_up, preferred_element_type=f32)
    square_part = jnp.sum(piecef * piecef, axis=1)
    up_total, square_total = lax.psum((up_part, square_part), "kv")
    scale_ffn = lax.rsqrt(square_total / width + EPSILON)[:, None]
    hidden = jnp.square(jax.nn.relu(up_total * scale_ffn)).astype(bf16)
    down_terms = jnp.dot(hidden, w_down, preferred_element_type=f32)
    ffn_summed = lax.psum_scatter(down_terms, "tp", scatter_dimension=1, tiled=True)
    layer_out = (mixed.astype(f32) + ffn_summed).astype(bf16)
    return (layer_out, cell_next, norm_next, max_next)


def solution(mesh):
    in_specs = (
        P(None, ("kv", "tp")),
        P(),
        P("kv", "tp"),
        P("kv", "tp"),
        P("kv", "tp"),
        P("kv", "tp"),
        P("kv", None),
        P(),
        P("kv", "tp", None),
        P("kv", None, None),
        P("kv", None),
        P(),
        P("tp", "kv"),
        P(),
        P("kv", "tp"),
        P("tp", "kv"),
    )
    out_specs = (P(None, ("kv", "tp")), P("kv", "tp", None), P("kv", None, None), P("kv", None))
    return jax.shard_map(
        per_device, mesh=mesh, in_specs=in_specs, out_specs=out_specs, check_vma=False
    )
```

profile of v0, /device:TPU:0, one launch (start us, length us, event | category | flops | bytes accessed | tf_op | source)
XLA Modules:
  0.0 254.1 jit_solution(9708847309321128957)
XLA Ops:
  7.3 14.7 %all_gather.15 = bf16[32,1024]{1,0:T(8,128)(2,1)S(1)} all-gather(bf16[32,128]{1,0:T(8,128)(2,1)} %param.16), channel_id=1, replica_groups=mesh['kv'=4,'tp'=8] {'tp'}, dimensions={1}, use_global_device_ids=true | all-gather | bytes 73728 | tf_op jit(solution)/shard_map/all_gather | solution.py:36
  22.0 0.7 dynamic_slice.9
  22.7 2.1 fusion.31
  24.9 2.1 fusion.29
  27.0 2.1 fusion.27
  29.1 2.1 fusion.35
  32.9 16.5 %all-reduce.6 = (f32[32]{0:T(128)S(1)}, f32[32,32]{1,0:T(8,128)S(1)}) all-reduce(f32[32]{0:T(128)S(1)} %fusion.5, f32[32,32]{1,0:T(8,128)S(1)} %fusion.33), channel_id=3, replica_groups=mesh['kv'=4,'tp'=8] {'kv'}, use_global_device_ids=true, to_apply=%region_2.0.clone | all-reduce | flops 1056 | bytes 8448
  49.7 5.4 %copy.26 = f32[8,512,256]{1,2,0:T(8,128)} copy(f32[8,512,256]{2,1,0:T(8,128)} %param.24) | data formatting | bytes 8388608 | tf_op args[8]
  55.1 0.8 dynamic_slice.10
  56.0 18.8 %all-reduce.13.cloned.1.call-done = (f32[32,512]{1,0:T(8,128)}, f32[32,512]{1,0:T(8,128)}, f32[32,512]{1,0:T(8,128)}, f32[32,512]{1,0:T(8,128)}) async-done(((f32[32,512]{1,0:T(8,128)}, f32[32,512]{1,0:T(8,128)}, f32[32,512]{1,0:T(8,128)}, f32[32,512]{1,0:T(8,128)}), (f32[32,512]{1,0:T(8,128)}, f32[32,512]{1,0:T(8,128)}, f32[32,512]{1,0:T(8,128)}, f32[32,512]{1,0:T(8,128)})) %all-reduce.13.cloned.1.call-update) | async-done | bytes 262160
  74.8 0.9 convolution_multiply_fusion
  75.6 0.8 fusion.37
  76.4 14.0 %all_gather.16 = bf16[8,4096]{1,0:T(8,128)(2,1)S(1)} all-gather(bf16[8,512]{1,0:T(8,128)(2,1)S(1)} %get-tuple-element.23), channel_id=1, replica_groups=mesh['kv'=4,'tp'=8] {'tp'}, dimensions={1}, use_global_device_ids=true | all-gather | bytes 73728 | tf_op jit(solution)/shard_map/all_gather | solution.py:59
  90.4 14.0 %all_gather.17 = bf16[8,4096]{1,0:T(8,128)(2,1)S(1)} all-gather(bf16[8,512]{1,0:T(8,128)(2,1)S(1)} %get-tuple-element.22), channel_id=1, replica_groups=mesh['kv'=4,'tp'=8] {'tp'}, dimensions={1}, use_global_device_ids=true | all-gather | bytes 73728 | tf_op jit(solution)/shard_map/all_gather | solution.py:58
  104.4 4.3 %fusion.1 = f32[8,512,256]{1,2,0:T(8,128)S(1)} fusion(f32[8,512,256]{1,2,0:T(8,128)} %copy.26, f32[8,512]{1,0:T(8,128)S(1)} %convolution_multiply_fusion, f32[8,512]{1,0:T(8,128)S(1)} %fusion.24, f32[8,16,256]{2,0,1:T(8,128)S(1)} %convert.2, s32[512]{0:T(512)S(1)} %add_select_fusion), kind=kOutput, calls=%fused_computation.3 | convolution fusion | flops 204513280 | bytes 8554496 | tf_op jit(solution)/shard_map/shd,rh->srd/dot_general | solution.py:76
  108.7 1.9 copy-done.1
  110.6 0.8 fusion
  111.4 0.8 multiply_reduce_fusion
  112.2 0.9 fusion.3
  113.0 8.1 %all_gather.18 = bf16[32,512]{1,0:T(8,128)(2,1)S(1)} all-gather(bf16[8,512]{1,0:T(8,128)(2,1)S(1)} %fusion.3), channel_id=1, replica_groups=mesh['kv'=4,'tp'=8] {'kv'}, dimensions={0}, use_global_device_ids=true | all-gather | bytes 40960 | tf_op jit(solution)/shard_map/all_gather | solution.py:86
  121.2 0.9 fusion.20
  122.3 14.8 %psum.21 = f32[32]{0:T(128)S(1)} all-reduce(f32[32]{0:T(128)S(1)} %fusion.14), channel_id=1, replica_groups=mesh['kv'=4,'tp'=8] {'tp'}, use_global_device_ids=true, to_apply=%region_11.12 | all-reduce | flops 32 | bytes 256 | tf_op jit(solution)/shard_map/psum | solution.py:88
  137.2 15.7 %reduce-scatter.3.cloned.1.call-done = f32[32,128]{1,0:T(8,128)} async-done(((f32[32,1024]{1,0:T(8,128)}), f32[32,128]{1,0:T(8,128)}) %reduce-scatter.3.cloned.1.call-update) | async-done | bytes 16400 | tf_op jit(solution)/shard_map/reduce_scatter | solution.py:93
  152.9 0.8 add_convert_fusion.1
  153.7 12.7 %all_gather.19 = bf16[32,1024]{1,0:T(8,128)(2,1)S(1)} all-gather(bf16[32,128]{1,0:T(8,128)(2,1)S(1)} %add_convert_fusion.1), channel_id=1, replica_groups=mesh['kv'=4,'tp'=8] {'tp'}, dimensions={1}, use_global_device_ids=true | all-gather | bytes 73728 | tf_op jit(solution)/shard_map/all_gather | solution.py:96
  166.3 3.7 %fusion.15 = f32[32,2048]{1,0:T(8,128)} fusion(bf16[1024,2048]{1,0:T(8,128)(2,1)} %param.30, bf16[32,1024]{1,0:T(8,128)(2,1)S(1)} %all_gather.19, f32[1024]{0:T(1024)S(1)} %dynamic-slice-done), kind=kOutput, calls=%fused_computation.28 | convolution fusion | flops 134316032 | bytes 4526080 | tf_op jit(solution)/shard_map/dot_general | solution.py:101
  170.3 10.0 %psum.23 = f32[32]{0:T(128)S(1)} all-reduce(f32[32]{0:T(128)S(1)} %fusion.7), channel_id=1, replica_groups=mesh['kv'=4,'tp'=8] {'kv'}, use_global_device_ids=true, to_apply=%region_14.15 | all-reduce | flops 32 | bytes 256 | tf_op jit(solution)/shard_map/psum | solution.py:103
  180.2 31.5 %all-reduce.11.cloned.1.call-done = f32[32,2048]{1,0:T(8,128)} async-done(((f32[32,2048]{1,0:T(8,128)}), f32[32,2048]{1,0:T(8,128)}) %all-reduce.11.cloned.1.call-update) | async-done | bytes 262160 | tf_op jit(solution)/shard_map/psum | solution.py:103
  211.7 3.8 %fusion.8 = f32[32,1024]{1,0:T(8,128)} fusion(bf16[2048,1024]{1,0:T(8,128)(2,1)} %param.31, f32[32,2048]{1,0:T(8,128)} %all-reduce.11.cloned.1.call-done, f32[32]{0:T(128)S(1)} %add_rsqrt_fusion), kind=kOutput, calls=%fused_computation.17 | convolution fusion | flops 134479872 | bytes 4587648 | tf_op jit(solution)/shard_map/dot_general | solution.py:106
  215.6 5.3 %copy.31 = f32[8,512,256]{2,1,0:T(8,128)} copy(f32[8,512,256]{1,2,0:T(8,128)} %copy-done.1) | data formatting | bytes 8388608
  220.9 25.3 %reduce-scatter.5.cloned.1.call-done = f32[32,128]{1,0:T(8,128)} async-done(((f32[32,1024]{1,0:T(8,128)}), f32[32,128]{1,0:T(8,128)}) %reduce-scatter.5.cloned.1.call-update) | async-done | bytes 16400 | tf_op jit(solution)/shard_map/reduce_scatter | solution.py:107
  246.2 1.3 add_convert_fusion
  (41 shorter events, 1.9 us)
Async XLA Ops:
  7.2 114.0 %copy-start = (bf16[512,1024]{1,0:T(8,128)(2,1)S(1)}, bf16[512,1024]{1,0:T(8,128)(2,1)}, u32[]{:S(2)}) copy-start(bf16[512,1024]{1,0:T(8,128)(2,1)} %param.28) | copy-start | bytes 3145732
  7.2 24.4 %copy-start.8 = (u32[32]{0:T(128)S(1)}, u32[32]{0:T(128)}, u32[]{:S(2)}) copy-start(u32[32]{0:T(128)} %constant.55) | copy-start | bytes 388
  7.2 24.3 %copy-start.3 = (bf16[1024,32]{0,1:T(8,128)(2,1)S(1)}, bf16[1024,32]{0,1:T(8,128)(2,1)}, u32[]{:S(2)}) copy-start(bf16[1024,32]{0,1:T(8,128)(2,1)} %param.22) | copy-start | bytes 196612
  7.2 42.3 %copy-start.5 = (f32[8,16]{1,0:T(8,128)S(1)}, f32[8,16]{1,0:T(8,128)}, u32[]{:S(2)}) copy-start(f32[8,16]{1,0:T(8,128)} %param.26) | copy-start | bytes 1540
  7.2 42.3 %copy-start.7 = (f32[16]{0:T(128)S(1)}, f32[16]{0:T(128)}, u32[]{:S(2)}) copy-start(f32[16]{0:T(128)} %param.23) | copy-start | bytes 196
  7.2 67.5 %all-reduce.13.cloned.1.call-start = ((), (), s32[]{:S(2)}) async-start(), calls=%async_computation.5 | async-start | bytes 524288
  31.3 121.6 %reduce-scatter.3.cloned.1.call-start = ((), (), s32[]{:S(2)}) async-start(), calls=%async_computation.2 | async-start | bytes 147456 | tf_op jit(solution)/shard_map/reduce_scatter | solution.py:93
  49.6 25.2 %copy-start.6 = (f32[8,16]{1,0:T(8,128)}, f32[8,16]{1,0:T(8,128)S(1)}, u32[]{:S(2)}) copy-start(f32[8,16]{1,0:T(8,128)S(1)} %get-tuple-element.21) | copy-start | bytes 1540
  108.7 1.9 copy-start.1
  108.7 2.7 %copy-start.2 = (f32[8,16,256]{2,1,0:T(8,128)S(1)}, f32[8,16,256]{2,1,0:T(8,128)}, u32[]{:S(2)}) copy-start(f32[8,16,256]{2,1,0:T(8,128)} %param.25) | copy-start | bytes 393220
  108.7 44.1 %copy-start.4 = (bf16[32,128]{1,0:T(8,128)(2,1)S(1)}, bf16[32,128]{1,0:T(8,128)(2,1)}, u32[]{:S(2)}) copy-start(bf16[32,128]{1,0:T(8,128)(2,1)} %param.16) | copy-start | bytes 24580
  108.7 57.6 %dynamic-slice-start = ((f32[4096]{0:T(1024)}, s32[]{:T(128)}), f32[1024]{0:T(1024)S(1)}, s32[]{:S(2)}) async-start(f32[4096]{0:T(1024)} %param.29, s32[]{:T(128)} %select_n.22), calls=%async_computation.6 | async-start | bytes 8704 | tf_op jit(solution)/shard_map/dynamic_slice | solution.py:99
  122.1 89.6 %all-reduce.11.cloned.1.call-start = ((), (), s32[]{:S(2)}) async-start(), calls=%async_computation.3 | async-start | bytes 524288 | tf_op jit(solution)/shard_map/psum | solution.py:103
  170.1 76.2 %reduce-scatter.5.cloned.1.call-start = ((), (), s32[]{:S(2)}) async-start(), calls=%async_computation.4 | async-start | bytes 147456 | tf_op jit(solution)/shard_map/reduce_scatter | solution.py:107
Sparse Core Ops, SparseCore 0:
  31.4 43.3 all-reduce.12
  122.3 30.5 reduce-scatter.2
  170.2 41.4 all-reduce.10
  215.7 30.5 reduce-scatter.4
where the time goes:
time: 255 us; the launch traced here: 254 us
  blocking collectives  105 us (41%)
  waiting for transfers between devices  91.4 us (36%)
  matrix products  24 us (9%)
  local copies, waits for them, and re-layouts  14.7 us (6%)
  between operations  14.6 us (6%)
  other arithmetic  4.42 us (2%)
    psum x1, waiting for transfers between devices, per_device(): up_total, square_total = lax.psum((up_part, square_part), 'kv')  31.5 us
    reduce_scatter x1, waiting for transfers between devices, per_device(): lax.psum_scatter(down_terms, 'tp', scatter_dimension=1, tiled=True)  25.3 us
    unnamed x5, waiting for transfers between devices  18.8 us
    unnamed x1, blocking collectives  16.5 us
    reduce_scatter x1, waiting for transfers between devices, per_device(): lax.psum_scatter(mix_terms, 'tp', scatter_dimension=1, tiled=True)  15.7 us
    psum x1, blocking collectives, per_device(): group_total = lax.psum(jnp.sum(readf * readf, axis=1), 'tp')  14.8 us
    all_gather x1, blocking collectives, per_device(): block_rows = lax.all_gather(tokens, 'tp', axis=1, tiled=True)  14.7 us
    all_gather x1, blocking collectives, per_device(): lax.all_gather(query_part, 'tp', axis=1, tiled=True)  14 us
  transfers between devices with their start and end apart: 4, of which 4 were waited for; matrix products, arithmetic and copies ran while one was open for 5% of the time, Pallas kernels for 0%

commit v1 on v0

--- a/solution.py
+++ b/solution.py
@@ -1,8 +1,11 @@
+import functools
 import math
 
 import jax
 import jax.numpy as jnp
 from jax import lax
+from jax.experimental import pallas as pl
+from jax.experimental.pallas import tpu as pltpu
 from jax.sharding import PartitionSpec as P
 
 EPSILON = 1e-06
@@ -109,6 +112,490 @@
     return (layer_out, cell_next, norm_next, max_next)
 
 
+MESH = pl.DeviceIdType.MESH
+LANES = 128
+SUBLANES = 8
+CHUNKS = 2
+
+
+def stack_rows(ref, count):
+    f32 = jnp.float32
+    rows = [ref[j].astype(f32) for j in range(count)]
+    return jnp.concatenate(rows, axis=0)
+
+
+def fused_kernel(
+    nk,
+    nt,
+    heads,
+    head_dim,
+    width,
+    tokens,
+    gain_mix,
+    w_query,
+    w_key,
+    w_value,
+    w_outgate,
+    w_gates,
+    forget_bias,
+    cell_state,
+    norm_state,
+    max_state,
+    gain_group,
+    w_mix,
+    gain_ffn,
+    w_up,
+    w_down,
+    layer_out,
+    rows_out,
+    gates_out,
+    keys_out,
+    tok_v,
+    gmix_v,
+    wq_v,
+    wk_v,
+    wv_v,
+    wo_v,
+    wg_v,
+    bias_v,
+    cell_v,
+    norm_v,
+    max_v,
+    ggroup_v,
+    wmix_v,
+    gffn_v,
+    wup_v,
+    wdown_v,
+    cell_b,
+    proj_part,
+    proj_recv,
+    gate_part,
+    gate_recv,
+    read_buf,
+    sq_part,
+    sq_recv,
+    mix_part,
+    mix_recv,
+    mixed_buf,
+    fsq_part,
+    fsq_recv,
+    up_part,
+    up_recv,
+    hid_buf,
+    down_part,
+    down_recv,
+    local_sem,
+    send_sem,
+    recv_sem,
+):
+    f32 = jnp.float32
+    bf16 = jnp.bfloat16
+    kv = lax.axis_index("kv")
+    tp = lax.axis_index("tp")
+    batch, cols = tokens.shape
+    seqs = batch // nk
+    block = cols * nt
+    vrows = wq_v.shape[1]
+    own_heads = vrows // head_dim
+    ffl = wup_v.shape[1]
+    chunk = ffl // CHUNKS
+
+    loads = {}
+
+    def load(name, source, target):
+        copy = pltpu.make_async_copy(source, target, local_sem.at[len(loads)])
+        copy.start()
+        loads[name] = copy
+
+    load("tok", tokens, tok_v.at[tp])
+    load("gmix", gain_mix, gmix_v)
+    load("wq", w_query, wq_v)
+    load("wk", w_key, wk_v)
+    load("wv", w_value, wv_v)
+    load("wo", w_outgate, wo_v)
+    load("wg", w_gates, wg_v)
+
+    barrier = pltpu.get_barrier_semaphore()
+    for d in range(1, nt):
+        pl.semaphore_signal(
+            barrier, inc=1, device_id={"tp": lax.rem(tp + d, nt)}, device_id_type=MESH
+        )
+    for d in range(1, nk):
+        pl.semaphore_signal(
+            barrier, inc=1, device_id={"kv": lax.rem(kv + d, nk)}, device_id_type=MESH
+        )
+    pl.semaphore_wait(barrier, nt + nk - 2)
+
+    used = [0]
+    sent = []
+
+    def exchange(axis, count, me, source, target):
+        copies = []
+        for d in range(1, count):
+            peer = lax.rem(me + d, count)
+            copy = pltpu.make_async_remote_copy(
+                src_ref=source(peer),
+                dst_ref=target,
+                send_sem=send_sem.at[used[0]],
+                recv_sem=recv_sem.at[used[0]],
+                device_id={axis: peer},
+                device_id_type=MESH,
+            )
+            copy.start()
+            used[0] += 1
+            copies.append(copy)
+        sent.extend(copies)
+        return copies
+
+    def arrive(copies):
+        for copy in copies:
+            copy.wait_recv()
+
+    def total(own, recv, me, count):
+        result = own[me].astype(f32)
+        for d in range(1, count):
+            result = result + recv[lax.rem(me + count - d, count)].astype(f32)
+        return result
+
+    got = exchange("tp", nt, tp, lambda peer: tokens, tok_v.at[tp])
+    load("cell", cell_state, cell_v)
+    load("norm", norm_state, norm_v)
+    load("max", max_state, max_v)
+    load("bias", forget_bias, bias_v)
+    load("ggroup", gain_group, ggroup_v)
+    load("gffn", gain_ffn, gffn_v)
+    load("wmix", w_mix, wmix_v)
+    load("wup", w_up, wup_v)
+    load("wdown", w_down, wdown_v)
+    loads["tok"].wait()
+    loads["gmix"].wait()
+    arrive(got)
+    blockf = jnp.concatenate([tok_v[j].astype(f32) for j in range(nt)], axis=1)
+    gain = gmix_v[:, pl.ds(pl.multiple_of(kv * block, LANES), block)]
+    normed = (blockf * gain).astype(bf16)
+    squares = jnp.sum(blockf * blockf, axis=1, keepdims=True)
+    loads["wg"].wait()
+    gates_p = lax.dot_general(
+        normed, wg_v[...], (((1,), (1,)), ((), ())), preferred_element_type=f32
+    )
+    squares_b = jnp.broadcast_to(squares, (batch, LANES))
+    for j in range(nk):
+        gate_part[j] = squares_b[j * seqs : (j + 1) * seqs]
+        gate_part[j, :, : 2 * heads] = gates_p[j * seqs : (j + 1) * seqs]
+    got_gates = exchange("kv", nk, kv, lambda peer: gate_part.at[peer], gate_recv.at[kv])
+    got_proj = []
+    for i, (name, weight) in enumerate((("wq", wq_v), ("wk", wk_v), ("wv", wv_v), ("wo", wo_v))):
+        loads[name].wait()
+        part = jnp.dot(normed, weight[...], preferred_element_type=f32)
+        for j in range(nk):
+            proj_part[i, j] = part[j * seqs : (j + 1) * seqs].astype(bf16)
+        got_proj.append(
+            exchange("kv", nk, kv, lambda peer, i=i: proj_part.at[i, peer], proj_recv.at[i, kv])
+        )
+
+    loads["cell"].wait()
+    for s in range(seqs):
+        cell_b[s] = cell_v[s].astype(bf16)
+    loads["norm"].wait()
+    loads["max"].wait()
+    loads["bias"].wait()
+
+    arrive(got_gates)
+    gsum = total(gate_part, gate_recv, kv, nk)
+    scale_in = lax.rsqrt(gsum[:, 2 * heads : 2 * heads + 1] / width + EPSILON)
+    scaled = gsum * scale_in
+    gate_in = scaled[:, :heads]
+    gate_forget = pltpu.roll(scaled, LANES - heads, 1)[:, :heads]
+    max_state_ = max_v[...]
+    log_forget = jax.nn.log_sigmoid(gate_forget + bias_v[...])
+    max_next = jnp.maximum(log_forget + max_state_, gate_in)
+    decay = jnp.exp(log_forget + max_state_ - max_next)
+    inflow = jnp.exp(gate_in - max_next)
+    gates_out[0] = max_next
+    gates_out[1] = decay
+    gates_out[2] = inflow
+    head_ids = lax.broadcasted_iota(jnp.int32, (seqs, heads), 1)
+
+    def own(values, h):
+        mine = jnp.where(head_ids == tp * own_heads + h, values, 0.0)
+        return jnp.sum(mine, axis=1, keepdims=True)
+
+    own_decay = [own(decay, h) for h in range(own_heads)]
+    own_inflow = [own(inflow, h) for h in range(own_heads)]
+    norm_ids = lax.broadcasted_iota(jnp.int32, (seqs, heads, head_dim), 1)
+    norm_own = [
+        jnp.sum(jnp.where(norm_ids == tp * own_heads + h, norm_v[...], 0.0), axis=1)
+        for h in range(own_heads)
+    ]
+
+    sums = []
+    for i in range(4):
+        arrive(got_proj[i])
+        sums.append(total(proj_part.at[i], proj_recv.at[i], kv, nk) * scale_in)
+    query = sums[0].astype(bf16)
+    key = sums[1].astype(bf16)
+    values = sums[2]
+    opened = jax.nn.sigmoid(sums[3])
+    keys_out[tp] = key
+    queryf = query.astype(f32)
+    keyf = key.astype(f32) / math.sqrt(head_dim)
+    row_ids = lax.broadcasted_iota(jnp.int32, (seqs, head_dim), 0)
+    reads = []
+    for h in range(own_heads):
+        span = slice(h * head_dim, (h + 1) * head_dim)
+        qh = queryf[:, span]
+        kh = keyf[:, span]
+        numer = jnp.zeros((seqs, head_dim), f32)
+        for s in range(seqs):
+            lhs = jnp.where(row_ids == s, qh, 0.0).astype(bf16)
+            numer += lax.dot_general(
+                lhs,
+                cell_b[s, span, :],
+                (((1,), (1,)), ((), ())),
+                preferred_element_type=f32,
+            )
+        gain_k = own_inflow[h] * kh
+        norm_h = own_decay[h] * norm_own[h] + gain_k
+        denom = jnp.maximum(jnp.abs(jnp.sum(norm_h * qh, axis=1, keepdims=True)), 1.0)
+        kq = jnp.sum(gain_k * qh, axis=1, keepdims=True)
+        numer = own_decay[h] * numer + values[:, span] * kq
+        reads.append((opened[:, span] * (numer / denom)).astype(bf16))
+        rows_out[0, :, span] = values[:, span]
+        rows_out[1, :, span] = gain_k
+        rows_out[2, :, span] = jnp.broadcast_to(own_decay[h], (seqs, head_dim))
+    read_buf[kv] = jnp.concatenate(reads, axis=1)
+    got = exchange("kv", nk, kv, lambda peer: read_buf.at[kv], read_buf.at[kv])
+    got_keys = exchange("tp", nt, tp, lambda peer: keys_out.at[tp], keys_out.at[tp])
+    loads["ggroup"].wait()
+    loads["wmix"].wait()
+    gain = ggroup_v[:, pl.ds(pl.multiple_of(tp * vrows, LANES), vrows)]
+    arrive(got)
+    readf = stack_rows(read_buf, nk)
+    groups = batch // SUBLANES
+    stride = LANES // groups
+    squares = jnp.sum(readf * readf, axis=1, keepdims=True)
+    lane_ids = lax.broadcasted_iota(jnp.int32, (SUBLANES, LANES), 1)
+    packed = jnp.zeros((SUBLANES, LANES), f32)
+    for a in range(groups):
+        packed = jnp.where(
+            lane_ids // stride == a, squares[a * SUBLANES : (a + 1) * SUBLANES], packed
+        )
+    sq_part[...] = packed
+    got_sq = exchange("tp", nt, tp, lambda peer: sq_part, sq_recv.at[tp])
+    grouped = (readf * gain).astype(bf16)
+    terms = jnp.dot(grouped, wmix_v[...], preferred_element_type=f32)
+    for j in range(nt):
+        mix_part[j] = terms[:, j * cols : (j + 1) * cols].astype(bf16)
+    got = exchange("tp", nt, tp, lambda peer: mix_part.at[peer], mix_recv.at[tp])
+    tokf = tok_v[tp].astype(f32)
+    arrive(got_sq)
+    for d in range(1, nt):
+        packed = packed + sq_recv[lax.rem(tp + nt - d, nt)]
+    scale_packed = lax.rsqrt(packed / (heads * head_dim) + EPSILON)
+    scale_group = jnp.concatenate(
+        [scale_packed[:, a * stride : a * stride + 1] for a in range(groups)], axis=0
+    )
+    arrive(got)
+    mixed = (tokf + total(mix_part, mix_recv, tp, nt) * scale_group).astype(bf16)
+    mixed_buf[tp] = mixed
+    got = exchange("tp", nt, tp, lambda peer: mixed_buf.at[tp], mixed_buf.at[tp])
+    loads["gffn"].wait()
+    loads["wup"].wait()
+    gain = gffn_v[:, pl.ds(pl.multiple_of(kv * block, LANES), block)]
+    arrive(got)
+    piecef = jnp.concatenate([mixed_buf[j].astype(f32) for j in range(nt)], axis=1)
+    normed = (piecef * gain).astype(bf16)
+    squares = jnp.broadcast_to(jnp.sum(piecef * piecef, axis=1, keepdims=True), (batch, LANES))
+    for j in range(nk):
+        fsq_part[j] = squares[j * seqs : (j + 1) * seqs]
+    got_fsq = exchange("kv", nk, kv, lambda peer: fsq_part.at[peer], fsq_recv.at[kv])
+    got_up = []
+    for c in range(CHUNKS):
+        part = jnp.dot(
+            normed, wup_v[:, c * chunk : (c + 1) * chunk], preferred_element_type=f32
+        )
+        for j in range(nk):
+            up_part[c, j] = part[j * seqs : (j + 1) * seqs].astype(bf16)
+        got_up.append(
+            exchange("kv", nk, kv, lambda peer, c=c: up_part.at[c, peer], up_recv.at[c, kv])
+        )
+    arrive(got_fsq)
+    square_total = total(fsq_part, fsq_recv, kv, nk)
+    scale_ffn = lax.rsqrt(square_total[:, :1] / width + EPSILON)
+    got_hid = []
+    for c in range(CHUNKS):
+        arrive(got_up[c])
+        up_total = total(up_part.at[c], up_recv.at[c], kv, nk)
+        hid_buf[c, kv] = jnp.square(jax.nn.relu(up_total * scale_ffn)).astype(bf16)
+        got_hid.append(
+            exchange("kv", nk, kv, lambda peer, c=c: hid_buf.at[c, kv], hid_buf.at[c, kv])
+        )
+    loads["wdown"].wait()
+    terms = jnp.zeros((batch, block), f32)
+    for c in range(CHUNKS):
+        arrive(got_hid[c])
+        hidden = stack_rows(hid_buf.at[c], nk).astype(bf16)
+        terms = terms + jnp.dot(
+            hidden, wdown_v[c * chunk : (c + 1) * chunk, :], preferred_element_type=f32
+        )
+    for j in range(nt):
+        down_part[j] = terms[:, j * cols : (j + 1) * cols].astype(bf16)
+    got = exchange("tp", nt, tp, lambda peer: down_part.at[peer], down_recv.at[tp])
+    arrive(got_keys)
+    arrive(got)
+    layer = mixed.astype(f32) + total(down_part, down_recv, tp, nt)
+    layer_out[...] = layer.astype(bf16)
+    for copy in sent:
+        copy.wait_send()
+
+
+def state_kernel(
+    heads,
+    head_dim,
+    layer,
+    rows,
+    gates,
+    keys,
+    cell_state,
+    norm_state,
+    layer_out,
+    cell_next,
+    norm_next,
+    max_next,
+    values_t,
+):
+    f32 = jnp.float32
+    s = pl.program_id(0)
+    vrows = rows.shape[2]
+    own_heads = vrows // head_dim
+
+    @pl.when(s == 0)
+    def _():
+        values_t[...] = jnp.transpose(rows[0])
+        layer_out[...] = layer[...]
+        max_next[...] = gates[0]
+        decay = gates[1]
+        inflow = gates[2]
+        for h in range(heads):
+            j, i = divmod(h, own_heads)
+            key = keys[j, :, i * head_dim : (i + 1) * head_dim].astype(f32)
+            key = key / math.sqrt(head_dim)
+            norm_next[:, h, :] = (
+                decay[:, h : h + 1] * norm_state[:, h, :] + inflow[:, h : h + 1] * key
+            )
+
+    lanes = lax.broadcasted_iota(jnp.int32, values_t.shape, 1)
+    column = jnp.sum(jnp.where(lanes == s, values_t[...], 0.0), axis=1, keepdims=True)
+    for h in range(own_heads):
+        span = slice(h * head_dim, (h + 1) * head_dim)
+        gain_k = rows[1, pl.ds(s, 1), span]
+        decay = rows[2, pl.ds(s, 1), span]
+        cell_next[0, span, :] = decay * cell_state[0, span, :] + column[span] * gain_k
+
+
+def fused_device(nk, nt, *args):
+    f32 = jnp.float32
+    bf16 = jnp.bfloat16
+    tokens, gain_mix = args[0], args[1]
+    w_gates = args[6]
+    forget_bias, cell_state, norm_state, max_state = args[7:11]
+    w_up = args[14]
+    width = gain_mix.shape[0]
+    heads = forget_bias.shape[0]
+    batch, cols = tokens.shape
+    seqs, vrows, head_dim = cell_state.shape
+    ffl = w_up.shape[1]
+    chunk = ffl // CHUNKS
+    block = cols * nt
+    vm = pltpu.VMEM
+    operands = list(args)
+    for i in (1, 7, 11, 13):
+        operands[i] = args[i].reshape(1, -1)
+    operands[6] = w_gates.T
+    landing = [vm(a.shape, a.dtype) for a in operands]
+    landing[0] = vm((nt, batch, cols), bf16)
+    transfers = (nt - 1) * 6 + (nk - 1) * (7 + 2 * CHUNKS)
+    scratch = landing + [
+        vm(cell_state.shape, bf16),
+        vm((4, nk, seqs, vrows), bf16),
+        vm((4, nk, seqs, vrows), bf16),
+        vm((nk, seqs, LANES), f32),
+        vm((nk, seqs, LANES), f32),
+        vm((nk, seqs, vrows), bf16),
+        vm((SUBLANES, LANES), f32),
+        vm((nt, SUBLANES, LANES), f32),
+        vm((nt, batch, cols), bf16),
+        vm((nt, batch, cols), bf16),
+        vm((nt, batch, cols), bf16),
+        vm((nk, seqs, LANES), f32),
+        vm((nk, seqs, LANES), f32),
+        vm((CHUNKS, nk, seqs, chunk), bf16),
+        vm((CHUNKS, nk, seqs, chunk), bf16),
+        vm((CHUNKS, nk, seqs, chunk), bf16),
+        vm((nt, batch, cols), bf16),
+        vm((nt, batch, cols), bf16),
+        pltpu.SemaphoreType.DMA((len(operands),)),
+        pltpu.SemaphoreType.DMA((transfers,)),
+        pltpu.SemaphoreType.DMA((transfers,)),
+    ]
+    layer, rows, gates, keys = pl.pallas_call(
+        functools.partial(fused_kernel, nk, nt, heads, head_dim, width),
+        name="fused_step",
+        out_shape=(
+            jax.ShapeDtypeStruct((batch, cols), bf16),
+            jax.ShapeDtypeStruct((3, seqs, vrows), f32),
+            jax.ShapeDtypeStruct((3, seqs, heads), f32),
+            jax.ShapeDtypeStruct((nt, seqs, vrows), bf16),
+        ),
+        in_specs=[pl.BlockSpec(memory_space=pl.ANY)] * len(operands),
+        out_specs=(pl.BlockSpec(memory_space=pltpu.VMEM),) * 4,
+        scratch_shapes=scratch,
+        compiler_params=pltpu.CompilerParams(
+            collective_id=0, has_side_effects=True, vmem_limit_bytes=56 * 1024 * 1024
+        ),
+    )(*operands)
+
+    def whole(array):
+        zeros = (0,) * len(array.shape)
+        return pl.BlockSpec(array.shape, lambda s: zeros)
+
+    step = pl.BlockSpec((1, vrows, head_dim), lambda s: (s, 0, 0))
+    layer_out, cell_next, norm_next, max_next = pl.pallas_call(
+        functools.partial(state_kernel, heads, head_dim),
+        name="state_update",
+        grid=(seqs,),
+        out_shape=(
+            jax.ShapeDtypeStruct((batch, cols), bf16),
+            jax.ShapeDtypeStruct(cell_state.shape, f32),
+            jax.ShapeDtypeStruct(norm_state.shape, f32),
+            jax.ShapeDtypeStruct(max_state.shape, f32),
+        ),
+        in_specs=[whole(layer), whole(rows), whole(gates), whole(keys), step, whole(norm_state)],
+        out_specs=(whole(layer), step, whole(norm_state), whole(max_state)),
+        scratch_shapes=[vm((vrows, seqs), f32)],
+    )(layer, rows, gates, keys, cell_state, norm_state)
+    return layer_out, cell_next, norm_next, max_next
+
+
+def device_step(nk, nt, *args):
+    tokens, cell_state = args[0], args[8]
+    batch, cols = tokens.shape
+    seqs, vrows, head_dim = cell_state.shape
+    ffl = args[14].shape[1]
+    fits = (
+        cols % LANES == 0
+        and vrows % head_dim == 0
+        and head_dim % LANES == 0
+        and seqs % SUBLANES == 0
+        and LANES % (batch // SUBLANES) == 0
+        and ffl % (CHUNKS * LANES) == 0
+        and 3 * args[7].shape[0] <= LANES
+    )
+    if fits:
+        return fused_device(nk, nt, *args)
+    return per_device(*args)
+
+
 def solution(mesh):
     in_specs = (
         P(None, ("kv", "tp")),
@@ -130,5 +617,6 @@
     )
     out_specs = (P(None, ("kv", "tp")), P("kv", "tp", None), P("kv", None, None), P("kv", None))
     return jax.shard_map(
-        per_device, mesh=mesh, in_specs=in_specs, out_specs=out_specs, check_vma=False
-    )
+        functools.partial(device_step, mesh.shape["kv"], mesh.shape["tp"]),
+        mesh=mesh, in_specs=in_specs, out_specs=out_specs, check_vma=False
+    )

time: 255 us -> 48.4 us (0.19)
  blocking collectives: 105 us -> 0 us
  waiting for transfers between devices: 91.4 us -> 0 us
  Pallas kernels: 0 us -> 47.5 us
  matrix products: 24 us -> 0 us
  local copies, waits for them, and re-layouts: 14.7 us -> 0 us
  between operations: 14.6 us -> 0.64 us
  other arithmetic: 4.42 us -> 0 us
    all_gather x5 -> x0, blocking collectives: 63.5 us -> none  [the longest x1 14.7 us: per_device(): block_rows = lax.all_gather(tokens, 'tp', axis=1, tiled=True)]
    pallas_call x0 -> x2, Pallas kernels: none -> 47.5 us  [the longest x1 40.1 us: fused_device(): pl.pallas_call(functools.partial(fused_kernel, nk, nt, heads, head_dim, w...]
    reduce_scatter x2 -> x0, waiting for transfers between devices: 41.1 us -> none  [the longest x1 25.3 us: per_device(): lax.psum_scatter(down_terms, 'tp', scatter_dimension=1, tiled=True)]
    psum x1 -> x0, waiting for transfers between devices: 31.5 us -> none  [per_device(): up_total, square_total = lax.psum((up_part, square_part), 'kv')]
    psum x2 -> x0, blocking collectives: 24.8 us -> none  [the longest x1 14.8 us: per_device(): group_total = lax.psum(jnp.sum(readf * readf, axis=1), 'tp')]
    dot_general x13 -> x0, matrix products: 24 us -> none  [the longest x5 8.67 us: per_device(): jnp.dot(normed, weight, preferred_element_type=f32)]
    unnamed x5 -> x0, waiting for transfers between devices: 18.8 us -> none
    unnamed x1 -> x0, blocking collectives: 16.5 us -> none
  transfers between devices with their start and end apart: 4 -> 0, of which waited for: 4 -> 0; matrix products, arithmetic and copies ran while one was open for 5% -> 0% of each run, Pallas kernels for 0% -> 0%
where the time goes in v1:
time: 48.4 us; the launch traced here: 48.2 us
  Pallas kernels  47.5 us (98%)
  between operations  0.64 us (1%)
    pallas_call x1, Pallas kernels, fused_device(): pl.pallas_call(functools.partial(fused_kernel, nk, nt, heads, head_dim, w...  40.1 us
    pallas_call x1, Pallas kernels, fused_device(): pl.pallas_call(functools.partial(state_kernel, heads, head_dim), name='st...  7.37 us

profile of v1, /device:TPU:0, one launch (start us, length us, event | category | flops | bytes accessed | tf_op | source)
XLA Modules:
  0.0 48.2 jit_solution(10364677850047460100)
XLA Ops:
  0.6 40.1 %fused_step.1 = (bf16[32,128]{1,0:T(8,128)(2,1)}, f32[3,8,512]{2,1,0:T(8,128)}, f32[3,8,16]{2,1,0:T(8,128)}, bf16[8,8,512]{2,1,0:T(8,128)(2,1)}) custom-call(bf16[32,128]{1,0:T(8,128)(2,1)} %tokens.1, f32[1,4096]{1,0:T(1,128)} %bitcast.6, bf16[1024,512]{1,0:T(8,128)(2,1)} %w_query.1, bf16[1024,512]{1,0:T(8,128)(2,1)} %w_key.1, bf16[1024,512]{1,0:T(8,128)(2,1)} %w_value.1, ...), custom_call_target="tpu_custom_call" | custom-call | tf_op jit(solution)/shard_map/fused_step/pallas_call | solution.py:541
  40.8 7.4 %state_update.1 = (bf16[32,128]{1,0:T(8,128)(2,1)}, f32[8,512,256]{2,1,0:T(8,128)}, f32[8,16,256]{2,1,0:T(8,128)}, f32[8,16]{1,0:T(8,128)}) custom-call(bf16[32,128]{1,0:T(8,128)(2,1)} %get-tuple-element.8.layer, f32[3,8,512]{2,1,0:T(8,128)} %get-tuple-element.9.rows, f32[3,8,16]{2,1,0:T(8,128)} %get-tuple-element.10.gates, ...), custom_call_target="tpu_custom_call" | custom-call | tf_op jit(solution)/shard_map/state_update/pallas_call | solution.py:563

commit v2 on v1

--- a/solution.py
+++ b/solution.py
@@ -116,6 +116,7 @@
 LANES = 128
 SUBLANES = 8
 CHUNKS = 2
+VMEM_BYTES = 67043328
 
 
 def stack_rows(ref, count):
@@ -147,9 +148,10 @@
     w_up,
     w_down,
     layer_out,
-    rows_out,
-    gates_out,
-    keys_out,
+    cell_out,
+    norm_out,
+    max_out,
+    keys_buf,
     tok_v,
     gmix_v,
     wq_v,
@@ -311,9 +313,7 @@
     max_next = jnp.maximum(log_forget + max_state_, gate_in)
     decay = jnp.exp(log_forget + max_state_ - max_next)
     inflow = jnp.exp(gate_in - max_next)
-    gates_out[0] = max_next
-    gates_out[1] = decay
-    gates_out[2] = inflow
+    max_out[...] = max_next
     head_ids = lax.broadcasted_iota(jnp.int32, (seqs, heads), 1)
 
     def own(values, h):
@@ -336,11 +336,12 @@
     key = sums[1].astype(bf16)
     values = sums[2]
     opened = jax.nn.sigmoid(sums[3])
-    keys_out[tp] = key
+    keys_buf[tp] = key
     queryf = query.astype(f32)
     keyf = key.astype(f32) / math.sqrt(head_dim)
     row_ids = lax.broadcasted_iota(jnp.int32, (seqs, head_dim), 0)
     reads = []
+    gain_keys = []
     for h in range(own_heads):
         span = slice(h * head_dim, (h + 1) * head_dim)
         qh = queryf[:, span]
@@ -360,12 +361,23 @@
         kq = jnp.sum(gain_k * qh, axis=1, keepdims=True)
         numer = own_decay[h] * numer + values[:, span] * kq
         reads.append((opened[:, span] * (numer / denom)).astype(bf16))
-        rows_out[0, :, span] = values[:, span]
-        rows_out[1, :, span] = gain_k
-        rows_out[2, :, span] = jnp.broadcast_to(own_decay[h], (seqs, head_dim))
+        gain_keys.append(gain_k)
     read_buf[kv] = jnp.concatenate(reads, axis=1)
     got = exchange("kv", nk, kv, lambda peer: read_buf.at[kv], read_buf.at[kv])
-    got_keys = exchange("tp", nt, tp, lambda peer: keys_out.at[tp], keys_out.at[tp])
+    got_keys = exchange("tp", nt, tp, lambda peer: keys_buf.at[tp], keys_buf.at[tp])
+    values_t = jnp.transpose(values)
+
+    def update(first, last):
+        for s in range(first, last):
+            for h in range(own_heads):
+                span = slice(h * head_dim, (h + 1) * head_dim)
+                cell_out[s, span, :] = (
+                    own_decay[h][s : s + 1] * cell_v[s, span, :]
+                    + values_t[span, s : s + 1] * gain_keys[h][s : s + 1]
+                )
+
+    third = seqs // 3
+    update(0, third)
     loads["ggroup"].wait()
     loads["wmix"].wait()
     gain = ggroup_v[:, pl.ds(pl.multiple_of(tp * vrows, LANES), vrows)]
@@ -388,6 +400,7 @@
         mix_part[j] = terms[:, j * cols : (j + 1) * cols].astype(bf16)
     got = exchange("tp", nt, tp, lambda peer: mix_part.at[peer], mix_recv.at[tp])
     tokf = tok_v[tp].astype(f32)
+    update(third, 2 * third)
     arrive(got_sq)
     for d in range(1, nt):
         packed = packed + sq_recv[lax.rem(tp + nt - d, nt)]
@@ -399,6 +412,7 @@
     mixed = (tokf + total(mix_part, mix_recv, tp, nt) * scale_group).astype(bf16)
     mixed_buf[tp] = mixed
     got = exchange("tp", nt, tp, lambda peer: mixed_buf.at[tp], mixed_buf.at[tp])
+    update(2 * third, seqs)
     loads["gffn"].wait()
     loads["wup"].wait()
     gain = gffn_v[:, pl.ds(pl.multiple_of(kv * block, LANES), block)]
@@ -442,6 +456,11 @@
         down_part[j] = terms[:, j * cols : (j + 1) * cols].astype(bf16)
     got = exchange("tp", nt, tp, lambda peer: down_part.at[peer], down_recv.at[tp])
     arrive(got_keys)
+    for h in range(heads):
+        j, i = divmod(h, own_heads)
+        key = keys_buf[j, :, i * head_dim : (i + 1) * head_dim].astype(f32)
+        key = key / math.sqrt(head_dim)
+        norm_out[:, h, :] = decay[:, h : h + 1] * norm_v[:, h, :] + inflow[:, h : h + 1] * key
     arrive(got)
     layer = mixed.astype(f32) + total(down_part, down_recv, tp, nt)
     layer_out[...] = layer.astype(bf16)
@@ -449,48 +468,15 @@
         copy.wait_send()
 
 
-def state_kernel(
-    heads,
-    head_dim,
-    layer,
-    rows,
-    gates,
-    keys,
-    cell_state,
-    norm_state,
-    layer_out,
-    cell_next,
-    norm_next,
-    max_next,
-    values_t,
-):
-    f32 = jnp.float32
-    s = pl.program_id(0)
-    vrows = rows.shape[2]
-    own_heads = vrows // head_dim
-
-    @pl.when(s == 0)
-    def _():
-        values_t[...] = jnp.transpose(rows[0])
-        layer_out[...] = layer[...]
-        max_next[...] = gates[0]
-        decay = gates[1]
-        inflow = gates[2]
-        for h in range(heads):
-            j, i = divmod(h, own_heads)
-            key = keys[j, :, i * head_dim : (i + 1) * head_dim].astype(f32)
-            key = key / math.sqrt(head_dim)
-            norm_next[:, h, :] = (
-                decay[:, h : h + 1] * norm_state[:, h, :] + inflow[:, h : h + 1] * key
-            )
-
-    lanes = lax.broadcasted_iota(jnp.int32, values_t.shape, 1)
-    column = jnp.sum(jnp.where(lanes == s, values_t[...], 0.0), axis=1, keepdims=True)
-    for h in range(own_heads):
-        span = slice(h * head_dim, (h + 1) * head_dim)
-        gain_k = rows[1, pl.ds(s, 1), span]
-        decay = rows[2, pl.ds(s, 1), span]
-        cell_next[0, span, :] = decay * cell_state[0, span, :] + column[span] * gain_k
+def store_kernel(layer, cell, norm, top, layer_out, cell_out, norm_out, max_out, sems):
+    seqs = cell.shape[0]
+    copies = [(cell.at[s], cell_out.at[s]) for s in range(seqs)]
+    copies += [(layer, layer_out), (norm, norm_out), (top, max_out)]
+    copies = [pltpu.make_async_copy(a, b, sems.at[i]) for i, (a, b) in enumerate(copies)]
+    for copy in copies:
+        copy.start()
+    for copy in copies:
+        copy.wait()
 
 
 def fused_device(nk, nt, *args):
@@ -538,43 +524,33 @@
         pltpu.SemaphoreType.DMA((transfers,)),
         pltpu.SemaphoreType.DMA((transfers,)),
     ]
-    layer, rows, gates, keys = pl.pallas_call(
+    results = (
+        ((batch, cols), bf16),
+        (cell_state.shape, f32),
+        (norm_state.shape, f32),
+        (max_state.shape, f32),
+    )
+    kept = 4 * batch * cols + 4 * cell_state.size + 4 * norm_state.size + 2**16
+    held = pl.pallas_call(
         functools.partial(fused_kernel, nk, nt, heads, head_dim, width),
         name="fused_step",
-        out_shape=(
-            jax.ShapeDtypeStruct((batch, cols), bf16),
-            jax.ShapeDtypeStruct((3, seqs, vrows), f32),
-            jax.ShapeDtypeStruct((3, seqs, heads), f32),
-            jax.ShapeDtypeStruct((nt, seqs, vrows), bf16),
-        ),
-        in_specs=[pl.BlockSpec(memory_space=pl.ANY)] * len(operands),
+        out_shape=tuple(vm(shape, dtype) for shape, dtype in results),
+        in_specs=[pl.BlockSpec(memory_space=pltpu.HBM)] * len(operands),
         out_specs=(pl.BlockSpec(memory_space=pltpu.VMEM),) * 4,
-        scratch_shapes=scratch,
+        scratch_shapes=[vm((nt, seqs, vrows), bf16)] + scratch,
         compiler_params=pltpu.CompilerParams(
-            collective_id=0, has_side_effects=True, vmem_limit_bytes=56 * 1024 * 1024
+            collective_id=0, has_side_effects=True, vmem_limit_bytes=VMEM_BYTES - kept
         ),
     )(*operands)
-
-    def whole(array):
-        zeros = (0,) * len(array.shape)
-        return pl.BlockSpec(array.shape, lambda s: zeros)
-
-    step = pl.BlockSpec((1, vrows, head_dim), lambda s: (s, 0, 0))
-    layer_out, cell_next, norm_next, max_next = pl.pallas_call(
-        functools.partial(state_kernel, heads, head_dim),
-        name="state_update",
-        grid=(seqs,),
-        out_shape=(
-            jax.ShapeDtypeStruct((batch, cols), bf16),
-            jax.ShapeDtypeStruct(cell_state.shape, f32),
-            jax.ShapeDtypeStruct(norm_state.shape, f32),
-            jax.ShapeDtypeStruct(max_state.shape, f32),
-        ),
-        in_specs=[whole(layer), whole(rows), whole(gates), whole(keys), step, whole(norm_state)],
-        out_specs=(whole(layer), step, whole(norm_state), whole(max_state)),
-        scratch_shapes=[vm((vrows, seqs), f32)],
-    )(layer, rows, gates, keys, cell_state, norm_state)
-    return layer_out, cell_next, norm_next, max_next
+    return pl.pallas_call(
+        store_kernel,
+        name="store_results",
+        out_shape=tuple(jax.ShapeDtypeStruct(shape, dtype) for shape, dtype in results),
+        in_specs=[pl.BlockSpec(memory_space=pltpu.VMEM)] * 4,
+        out_specs=(pl.BlockSpec(memory_space=pl.ANY),) * 4,
+        scratch_shapes=[pltpu.SemaphoreType.DMA((seqs + 3,))],
+        compiler_params=pltpu.CompilerParams(vmem_limit_bytes=16 * 1024 * 1024),
+    )(*held)
 
 
 def device_step(nk, nt, *args):

time: 48.4 us -> 42.5 us (0.88)
  Pallas kernels: 47.5 us -> 41.7 us
    pallas_call x1, Pallas kernels: 7.37 us -> 2.14 us  [fused_device(): pl.pallas_call(store_kernel, name='store_results', out_shape=tuple((jax.S...]
    pallas_call x1, Pallas kernels: 40.1 us -> 39.6 us  [fused_device(): pl.pallas_call(functools.partial(fused_kernel, nk, nt, heads, head_dim, w...]
where the time goes in v2:
time: 42.5 us; the launch traced here: 42.4 us
  Pallas kernels  41.7 us (98%)
  between operations  0.65 us (2%)
    pallas_call x1, Pallas kernels, fused_device(): pl.pallas_call(functools.partial(fused_kernel, nk, nt, heads, head_dim, w...  39.6 us
    pallas_call x1, Pallas kernels, fused_device(): pl.pallas_call(store_kernel, name='store_results', out_shape=tuple((jax.S...  2.14 us

profile of v2, /device:TPU:0, one launch (start us, length us, event | category | flops | bytes accessed | tf_op | source)
XLA Modules:
  0.0 42.4 jit_solution(7828243286146687454)
XLA Ops:
  0.6 39.6 %fused_step.1 = (bf16[32,128]{1,0:T(8,128)(2,1)S(1)}, f32[8,512,256]{2,1,0:T(8,128)S(1)}, f32[8,16,256]{2,1,0:T(8,128)S(1)}, f32[8,16]{1,0:T(8,128)S(1)}) custom-call(bf16[32,128]{1,0:T(8,128)(2,1)} %tokens.1, f32[1,4096]{1,0:T(1,128)} %bitcast.6, bf16[1024,512]{1,0:T(8,128)(2,1)} %w_query.1, bf16[1024,512]{1,0:T(8,128)(2,1)} %w_key.1, ...), custom_call_target="tpu_custom_call" | custom-call | tf_op jit(solution)/shard_map/fused_step/pallas_call | solution.py:534
  40.2 2.1 %store_results.1 = (bf16[32,128]{1,0:T(8,128)(2,1)}, f32[8,512,256]{2,1,0:T(8,128)}, f32[8,16,256]{2,1,0:T(8,128)}, f32[8,16]{1,0:T(8,128)}) custom-call(bf16[32,128]{1,0:T(8,128)(2,1)S(1)} %get-tuple-element.8.layer, f32[8,512,256]{2,1,0:T(8,128)S(1)} %get-tuple-element.9.cell, f32[8,16,256]{2,1,0:T(8,128)S(1)} %get-tuple-element.10.norm, ...), custom_call_target="tpu_custom_call" | custom-call | tf_op jit(solution)/shard_map/store_results/pallas_call | solution.py:545
